TPU v7x, 32 devices: a whole 2x2x4 slice. The times are simulated.
32 devices in a mesh: grp: 2 (over y), sp: 4 (over z), tp: 4 (over x, core).
Axes of the slice: x: 2, y: 2, z: 4, core: 2. Of those that a mesh axis runs over, the one named last changes fastest.
Arguments:
- tokens: bfloat16 [3072, 4096], P(('grp', 'sp'), 'tp'), parts along dimension 0, may hold values from -6 to 6
- proj_b: bfloat16 [2, 4096, 2048], P(None, 'sp', 'tp'), may hold values from -0.09375 to 0.09375
- proj_c: bfloat16 [2, 4096, 2048], P(None, 'sp', 'tp'), may hold values from -0.09375 to 0.09375
- proj_x: bfloat16 [2, 4096, 2048], P(None, 'sp', 'tp'), may hold values from -0.09375 to 0.09375
- proj_out: bfloat16 [2, 2048, 4096], P(None, 'sp', 'tp'), may hold values from -1 to 1
- conv_taps: float32 [2, 3, 2048], P(None, None, 'tp'), may hold values from -3 to 3
- ln_gain: float32 [2, 4096], P(None, 'tp'), may hold values from 0.1 to 1.9
- ln_bias: float32 [2, 4096], P(None, 'tp'), may hold values from -2 to 2
Outputs:
- result: bfloat16 [3072, 4096], P(('grp', 'sp'), 'tp'), parts along dimension 0
There are 2 independent parts, one for each index of `grp`. A program takes and returns all parts, laid end to end along the dimension named above; an argument that names none is the same for every part. Nothing has to cross between parts.
All inputs are finite; a program needn't handle non-finite values.
Results may differ from a plain program's by a relative error of at most 0.012.
Values may be sent and summed in bfloat16 or wider, within the bound.
A program may use at most 128 MiB of HBM per device.

v0:
```python
import jax
import jax.numpy as jnp
from jax import lax
from jax.experimental import pallas as pl
from jax.experimental.pallas import tpu as pltpu
from jax.sharding import PartitionSpec as P


LAYERS = 2


norm_eps = 1e-05


def from_behind(block, axis, distance):
    devices = range(lax.axis_size(axis))
    route = [(i - distance, i) for i in devices if i - distance in devices]
    return lax.ppermute(block, axis, route)


def along_line(block, axis, earlier):
    size = lax.axis_size(axis)
    blocks, latest = [(0, block)], []
    for side, step in enumerate((1, -1)):
        moving = block
        if earlier:
            moving, _ = lax.optimization_barrier((moving, earlier[side]))
        hops = []
        for hop in range(1, size):
            start = range(hop - 1, size - 1) if step == 1 else range(1, size - hop + 1)
            moving = lax.ppermute(moving, axis, [(i, i + step) for i in start])
            hops.append((-step * hop, moving))
        latest.append(hops[max(len(hops) - 2, 0)][1])
        blocks += hops
    return sorted(blocks, key=lambda b: abs(b[0])), latest


def dot_by_blocks(left, blocks, here, size):
    total = None
    for offset, block in blocks:
        depth = block.shape[0]
        owner = jnp.clip(here + offset, 0, size - 1)
        columns = lax.dynamic_slice_in_dim(left, owner * depth, depth, 1)
        term = jnp.dot(columns, block, preferred_element_type=jnp.float32)
        total = term if total is None else total + term
    return total


def local(tokens, proj_b, proj_c, proj_x, proj_out, conv_taps, ln_gain, ln_bias):
    residual_scale = (2.0 * LAYERS) ** 0.25
    parts = lax.axis_size("grp")
    me = lax.axis_index("grp")
    rows = tokens.shape[0]
    wide = proj_b.shape[2] // parts
    out_wide = proj_out.shape[2] // parts

    def mine(array, width):
        return lax.dynamic_slice_in_dim(array, me * width, width, array.ndim - 1)

    slabs, here = lax.axis_size("sp"), lax.axis_index("sp")
    weights = []
    earlier = None
    for layer_index in range(LAYERS):
        ins = jnp.concatenate(
            [mine(w[layer_index], wide) for w in (proj_b, proj_c, proj_x)], axis=1
        )
        ins, earlier = along_line(ins, "sp", earlier)
        outs, earlier = along_line(mine(proj_out[layer_index], out_wide), "sp", earlier)
        weights.append((ins, outs))
    taps, gain, bias = mine(conv_taps, wide), mine(ln_gain, out_wide), mine(ln_bias, out_wide)
    swapped = lax.all_to_all(
        tokens.reshape(rows, parts, out_wide), "grp", split_axis=1, concat_axis=0, tiled=False
    )
    hidden = swapped.reshape(parts * rows, out_wide)
    reach = taps.shape[1] - 1
    for layer_index in range(LAYERS):
        whole_in, whole_out = weights[layer_index]
        gathered = lax.all_gather(hidden, ("tp", "grp"), axis=1, tiled=True)
        acc = dot_by_blocks(gathered, whole_in, here, slabs)
        acc = lax.optimization_barrier(acc.astype(jnp.bfloat16)).astype(jnp.float32)
        out_gate, in_gate, values = (acc[:, i * wide : (i + 1) * wide] for i in range(3))
        gated_in = (in_gate * values).reshape(parts, rows, wide)
        fringe = from_behind(gated_in[:, rows - reach :], "sp", 1)
        padded = jnp.concatenate([fringe, gated_in], 1)
        conv_out = jnp.zeros_like(gated_in)
        for tap_index in range(reach + 1):
            conv_out = (
                conv_out + taps[layer_index, tap_index] * padded[:, tap_index : tap_index + rows]
            )
        branch = (out_gate * conv_out.reshape(parts * rows, wide)).astype(jnp.bfloat16)
        all_branch = lax.all_gather(branch, ("tp", "grp"), axis=1, tiled=True)
        acc_out = dot_by_blocks(all_branch, whole_out, here, slabs)
        mixed = lax.optimization_barrier(acc_out.astype(jnp.bfloat16))
        summed = residual_scale * hidden.astype(jnp.float32) + mixed.astype(jnp.float32)
        own_mean = jnp.mean(summed, axis=1)
        own_spread = jnp.mean(jnp.square(summed - own_mean[:, None]), axis=1)
        stats = lax.all_gather(jnp.stack([own_mean, own_spread]), ("tp", "grp"), axis=0)
        mean = jnp.mean(stats[:, 0], axis=0)
        variance = jnp.mean(stats[:, 1] + jnp.square(stats[:, 0] - mean), axis=0)[:, None]
        centered = summed - mean[:, None]
        hidden = (
            centered * lax.rsqrt(variance + norm_eps) * gain[layer_index] + bias[layer_index]
        ).astype(jnp.bfloat16)
    back = lax.all_to_all(
        hidden.reshape(parts, rows, out_wide), "grp", split_axis=0, concat_axis=1, tiled=False
    )
    return back.reshape(rows, parts * out_wide)


MESH = pl.DeviceIdType.MESH
CHUNKS = 4
HALO = 32
VMEM_BYTES = 63 * 2**20


def multiple(value, of):
    return pl.multiple_of(value, of)


def tile_rows(rows, most):
    return max(n for n in range(16, most + 1, 16) if rows % n == 0)


def mixer_kernel(
    tokens, proj_b, proj_c, proj_x, proj_out, conv_taps, ln_gain, ln_bias, out,
    hidden, raw, branch, w_in, w_out, acc, carry, stage, final, scales, own_scales, stats,
    local_sem, w_send, w_recv, ag_send, ag_recv, small_send, small_recv,
):
    f32, bf16 = jnp.float32, jnp.bfloat16
    residual_scale = (2.0 * LAYERS) ** 0.25
    g, s, t = (lax.axis_index(a) for a in ("grp", "sp", "tp"))
    parts, _, lanes = (lax.axis_size(a) for a in ("grp", "sp", "tp"))
    x, c = t // 2, t % 2
    rows, ow = tokens.shape
    kin, kout = proj_b.shape[1], proj_out.shape[1]
    wide, owide = proj_b.shape[2] // parts, ow // parts
    reach = conv_taps.shape[1] - 1
    part_rows = HALO + 2 * rows
    chunk_rows = parts * part_rows // CHUNKS
    half = s // 2
    base, end, mid = 2 * half, 3 * half, 1 + half
    other, far = 2 - half, 3 - 3 * half
    projections = (proj_b, proj_c, proj_x)
    kc = kin // 2

    def copy(src, dst, send, recv, device):
        return pltpu.make_async_remote_copy(src, dst, send, recv, device_id=device, device_id_type=MESH)

    def piece(layer, block, k):
        if k == 2:
            return w_out.at[layer, pl.ds(multiple(block * kout, kout), kout), :]
        return w_in.at[layer, pl.ds(multiple(block * kin + k * kc, kc), kc), :]

    def send_own(layer, k, device, row):
        sems = (w_send.at[row, layer * 3 + k], w_recv.at[row, layer * 3 + k])
        if k == 2:
            src = proj_out.at[layer, :, pl.ds(multiple(g * owide, owide), owide)]
            copy(src, piece(layer, s, k), *sems, device).start()
        else:
            for j, w in enumerate(projections):
                src = w.at[layer, pl.ds(k * kc, kc), pl.ds(multiple(g * wide, wide), wide)]
                dst = w_in.at[layer, pl.ds(multiple(s * kin + k * kc, kc), kc), pl.ds(j * wide, wide)]
                copy(src, dst, *sems, device).start()

    def w_wait(layer, k, row, block, sent=False):
        ref = piece(layer, block, k)
        c_ = copy(ref, ref, w_send.at[row, layer * 3 + k], w_recv.at[row, layer * 3 + k], (g, s, t))
        c_.wait_send() if sent else c_.wait_recv()

    def relay(layer, k):
        w_wait(layer, k, 0, end)
        ref = piece(layer, end, k)
        copy(ref, ref, w_send.at[2, layer * 3 + k], w_recv.at[2, layer * 3 + k], (g, other, t)).start()

    pieces = [(layer, k) for layer in range(LAYERS) for k in range(3)]

    def token_rows(index):
        return pl.ds(multiple(g * part_rows + HALO + index * rows, 16), rows)

    own_columns = pl.ds(multiple(t * ow + g * owide, owide), owide)

    def final_half(gg):
        return final.at[:, pl.ds(multiple(gg * owide, owide), owide)]

    @pl.when(s == end)
    def _():
        slab = hidden.at[token_rows(end - base), pl.ds(multiple(t * ow, ow), ow)]
        copy(tokens, slab, small_send.at[0], small_recv.at[0], (g, mid, t)).start()
        for i, (layer, k) in enumerate(pieces):
            if i >= 2:
                w_wait(*pieces[i - 2], 0, s, sent=True)
            send_own(layer, k, (g, mid, t), 0)
        for layer, k in pieces[-2:]:
            w_wait(layer, k, 0, s, sent=True)
        copy(tokens, slab, small_send.at[0], small_recv.at[0], (g, mid, t)).wait_send()
        for gg in range(parts):
            copy(final_half(gg), final_half(gg), small_send.at[2], small_recv.at[8 + gg], (g, s, t)).wait_recv()

    @pl.when(s == mid)
    def _():
        there = (g, other, t)
        yu, xu = g + c * (1 - 2 * g), x + (1 - c) * (1 - 2 * x)
        yv, xv = g + (1 - c) * (1 - 2 * g), x + c * (1 - 2 * x)
        up, vp, pp = (yu, mid, 2 * xu + c), (yv, mid, 2 * xv + c), (g, mid, 2 * x + 1 - c)
        diagonal = (1 - g, mid, 2 * (1 - x) + c)
        me = (g, mid, t)

        for k in range(2):
            send_own(0, k, there, 1)
        mine = hidden.at[token_rows(mid - base), pl.ds(multiple(t * ow, ow), ow)]
        pltpu.make_async_copy(tokens, mine, local_sem.at[0]).start()
        for layer in range(LAYERS):
            for j, w in enumerate(projections):
                pltpu.make_async_copy(
                    w.at[layer, :, pl.ds(multiple(g * wide, wide), wide)],
                    w_in.at[layer, pl.ds(multiple(s * kin, kin), kin), pl.ds(j * wide, wide)],
                    local_sem.at[1 + layer],
                ).start()
            pltpu.make_async_copy(
                proj_out.at[layer, :, pl.ds(multiple(g * owide, owide), owide)],
                piece(layer, s, 2),
                local_sem.at[1 + LAYERS + layer],
            ).start()

        edge = hidden.at[pl.ds(multiple(g * part_rows, 16), HALO), pl.ds(multiple(t * ow, ow), ow)]
        edge_copy = copy(tokens.at[pl.ds(rows - HALO, HALO), :], edge, small_send.at[1], small_recv.at[1], there)

        @pl.when(half == 0)
        def _():
            edge_copy.start()
            edge[...] = jnp.zeros_like(edge)

        own_scales[0:1, :] = ln_gain[0:1, :]
        own_scales[1:2, :] = ln_bias[0:1, :]
        scales[0:2, pl.ds(multiple(t * ow, ow), ow)] = own_scales[0:2, :]
        for k in range(1, lanes):
            copy(
                own_scales, scales.at[:, pl.ds(multiple(t * ow, ow), ow)],
                small_send.at[4 + k], small_recv.at[4 + k], (g, s, (t + k) % lanes),
            ).start()

        def gather(buffer, region, family, produce, consume, unroll=False):
            def at(device, i):
                return buffer.at[region(device[0], device[2], i)]

            def transfer(owner, i, role, kind, device):
                ref = at(owner, i)
                return copy(ref, ref, ag_send.at[family, i, kind], ag_recv.at[family, i, role], device)

            def arrived(i, role):
                transfer(me, i, role, 0, me).wait_recv()

            def send(i):
                transfer(me, i, 0, 0, up).start()
                transfer(me, i, 1, 1, vp).start()
                transfer(me, i, 3, 2, pp).start()

            def step(i):
                arrived(i, 0)
                transfer(up, i, 2, 4, vp).start()
                transfer(up, i, 4, 3, pp).start()
                arrived(i, 1)
                transfer(vp, i, 5, 5, pp).start()
                arrived(i, 2)
                transfer(diagonal, i, 6, 6, pp).start()
                for role in range(3, 7):
                    arrived(i, role)
                consume(i)

            produce(0)
            send(0)
            if unroll:
                for i in range(CHUNKS):
                    if i + 1 < CHUNKS:
                        produce(i + 1)
                        send(i + 1)
                    step(i)
            else:
                @pl.loop(0, CHUNKS)
                def _(i):
                    @pl.when(i + 1 < CHUNKS)
                    def _():
                        produce(i + 1)
                        send(i + 1)

                    step(i)

            @pl.loop(0, CHUNKS)
            def _(i):
                for kind in range(7):
                    transfer(me, i, 0, kind, me).wait_send()

        def row_chunk(i):
            return pl.ds(multiple(i * chunk_rows, 16), chunk_rows)

        def nothing(i):
            pass

        def token_hook(i):
            if i in (1, 2):
                relay(0, i - 1)
            if i == 2:
                send_own(0, 2, there, 1)

        pltpu.make_async_copy(tokens, mine, local_sem.at[0]).wait()
        theirs = hidden.at[token_rows(end - base), pl.ds(multiple(t * ow, ow), ow)]
        copy(theirs, theirs, small_send.at[0], small_recv.at[0], me).wait_recv()

        @pl.when(half == 1)
        def _():
            edge_copy.wait_recv()

        qw = ow // CHUNKS
        gather(
            hidden,
            lambda gg, tt, i: (
                pl.ds(multiple(gg * part_rows, 16), part_rows),
                pl.ds(multiple(tt * ow + i * qw, qw), qw),
            ),
            0, nothing, token_hook, unroll=True,
        )

        def accumulate(layer, start, depth, i, first=False):
            at_rows = row_chunk(i)
            term = jnp.dot(
                hidden[at_rows, pl.ds(multiple(start, kc), depth)],
                w_in[layer, pl.ds(multiple(start, kc), depth), :],
                preferred_element_type=f32,
            )
            acc[at_rows, :] = term if first else acc[at_rows, :] + term

        def wait_near_in(layer):
            ref = w_in.at[layer, pl.ds(multiple(s * kin, kin), kin), :]
            pltpu.make_async_copy(ref, ref, local_sem.at[1 + layer]).wait()

        def near_in(layer, i):
            accumulate(layer, base * kin, 2 * kin, i, first=True)

        def far_in(layer):
            for row, block in ((1, other), (2, far)):
                for k in range(2):
                    w_wait(layer, k, row, block)

                    @pl.loop(0, CHUNKS)
                    def _(i):
                        accumulate(layer, block * kin + k * kc, kc, i)

        tr = tile_rows(chunk_rows, 96)

        def gate(layer, i):
            taps = [
                conv_taps[layer, k : k + 1, pl.ds(multiple(g * wide, wide), wide)] for k in range(reach + 1)
            ]
            row_of = lax.broadcasted_iota(jnp.int32, (tr, wide), 0)

            @pl.loop(0, chunk_rows // tr)
            def _(q):
                start = multiple(i * chunk_rows + q * tr, 16)
                position = start % part_rows
                sums = acc[pl.ds(start, tr), :].astype(bf16).astype(f32)
                out_gate, in_gate, values = (sums[:, j * wide : (j + 1) * wide] for j in range(3))
                gated = in_gate * values
                gated = jnp.where(row_of < HALO * (1 - half) - position, 0.0, gated)
                before = jnp.where(position == 0, 0.0, carry[...])
                conv = jnp.zeros_like(gated)
                for k in range(reach + 1):
                    shift = reach - k
                    moved = gated
                    if shift:
                        moved = pltpu.roll(gated, shift, 0)
                        for j in range(shift):
                            moved = jnp.where(row_of == j, before[8 - shift + j : 8 - shift + j + 1, :], moved)
                    conv = conv + taps[k] * moved
                carry[...] = gated[tr - 8 :, :]
                branch[pl.ds(start, tr), pl.ds(multiple(t * parts * wide + g * wide, wide), wide)] = (
                    out_gate * conv
                ).astype(bf16)

        def branch_region(gg, tt, i):
            return row_chunk(i), pl.ds(multiple(tt * parts * wide + gg * wide, wide), wide)

        def sum_region(gg, tt, i):
            return row_chunk(i), pl.ds(multiple(tt * ow + gg * owide, owide), owide)

        def wait_out(layer):
            ref = piece(layer, s, 2)
            pltpu.make_async_copy(ref, ref, local_sem.at[1 + LAYERS + layer]).wait()
            for row, block in ((1, other), (2, far)):
                w_wait(layer, 2, row, block)

        def mix(layer, at_rows):
            mixed = jnp.dot(branch[at_rows, :], w_out[layer], preferred_element_type=f32)
            kept = hidden[at_rows, own_columns].astype(f32)
            return (residual_scale * kept + mixed.astype(bf16).astype(f32)).astype(bf16)

        def produce_sum(i):
            raw[row_chunk(i), own_columns] = mix(0, row_chunk(i))

        def normalise(i):
            @pl.loop(0, chunk_rows // 16)
            def _(q):
                at_rows = pl.ds(multiple(i * chunk_rows + q * 16, 16), 16)
                summed = raw[at_rows, :].astype(f32)
                mean = jnp.mean(summed, axis=1, keepdims=True)
                centered = summed - mean
                variance = jnp.mean(centered * centered, axis=1, keepdims=True)
                hidden[at_rows, :] = (
                    centered * lax.rsqrt(variance + norm_eps) * scales[0:1, :] + scales[1:2, :]
                ).astype(bf16)

        def consume_sum(i):
            normalise(i)
            near_in(1, i)

        wait_near_in(0)

        @pl.loop(0, CHUNKS)
        def _(i):
            near_in(0, i)

        relay(0, 2)
        for k in range(2):
            send_own(1, k, there, 1)
        far_in(0)
        gather(branch, branch_region, 1, lambda i: gate(0, i), nothing)
        for k in range(2):
            relay(1, k)
        send_own(1, 2, there, 1)
        for k in range(1, lanes):
            copy(
                own_scales, scales.at[:, pl.ds(multiple(((t + lanes - k) % lanes) * ow, ow), ow)],
                small_send.at[4 + k], small_recv.at[4 + k], me,
            ).wait()
        wait_out(0)
        wait_near_in(1)
        gather(raw, sum_region, 0, produce_sum, consume_sum)
        relay(1, 2)
        far_in(1)
        gather(branch, branch_region, 1, lambda i: gate(1, i), nothing)
        wait_out(1)

        def result_copy(j):
            p = (g + 1 + j // 2) % 2
            to = end + (j % 2) * (mid - end)
            return p, to, copy(
                stage.at[j], final_half(g), small_send.at[12 + j], small_recv.at[8 + g], (p, to, t)
            )

        @pl.loop(0, 4)
        def _(j):
            p, to, result = result_copy(j)
            stage[j] = mix(1, pl.ds(multiple(p * part_rows + HALO + (to - base) * rows, 16), rows))

            @pl.when(j < 3)
            def _():
                result.start()

        final[:, pl.ds(multiple(g * owide, owide), owide)] = stage[3]
        for j in range(3):
            result_copy(j)[2].wait_send()
        for layer, k in pieces:
            w_wait(layer, k, 1, s, sent=True)
            w_wait(layer, k, 2, end, sent=True)

        @pl.when(half == 0)
        def _():
            edge_copy.wait_send()

        copy(final_half(1 - g), final_half(1 - g), small_send.at[2], small_recv.at[8 + 1 - g], me).wait_recv()

    lane = lax.broadcasted_iota(jnp.int32, (128, 128), 1)
    line = lax.broadcasted_iota(jnp.int32, (128, 128), 0)

    @pl.loop(0, rows // 128)
    def _(b):
        at_rows = pl.ds(multiple(b * 128, 128), 128)
        summed = final[at_rows, :].astype(f32)
        mean = jnp.mean(summed, axis=1, keepdims=True)
        spread = jnp.mean(jnp.square(summed - mean), axis=1, keepdims=True)
        packed = jnp.where(lane == 0, mean, jnp.where(lane == 1, spread, 0.0))
        stats[t, :, at_rows] = packed.T[0:8, :]

    def stat_copy(k, owner):
        return copy(
            stats.at[owner], stats.at[owner], small_send.at[4 + k], small_recv.at[16 + k], (g, s, (t + k) % lanes)
        )

    for k in range(1, lanes):
        stat_copy(k, t).start()
    for k in range(1, lanes):
        stat_copy(k, (t + lanes - k) % lanes).wait()

    @pl.loop(0, rows // 128)
    def _(b):
        at_rows = pl.ds(multiple(b * 128, 128), 128)
        means = [stats[i, 0:1, at_rows] for i in range(lanes)]
        mean = sum(means) / lanes
        variance = sum(stats[i, 1:2, at_rows] + jnp.square(means[i] - mean) for i in range(lanes)) / lanes
        packed = jnp.where(line == 0, mean, jnp.where(line == 1, lax.rsqrt(variance + norm_eps), 0.0)).T
        centered = final[at_rows, :].astype(f32) - packed[:, 0:1]
        out[at_rows, :] = (
            centered * packed[:, 1:2] * ln_gain[LAYERS - 1 : LAYERS, :] + ln_bias[LAYERS - 1 : LAYERS, :]
        ).astype(bf16)


def mixer(tokens, proj_b, proj_c, proj_x, proj_out, conv_taps, ln_gain, ln_bias):
    parts, slabs, lanes = (lax.axis_size(a) for a in ("grp", "sp", "tp"))
    f32, bf16 = jnp.float32, jnp.bfloat16
    rows, ow = tokens.shape
    depth, channels = slabs * proj_b.shape[1], slabs * proj_out.shape[1]
    wide, owide = proj_b.shape[2] // parts, ow // parts
    total = parts * (HALO + 2 * rows)
    dma = pltpu.SemaphoreType.DMA
    anywhere, vmem = pl.BlockSpec(memory_space=pl.ANY), pl.BlockSpec(memory_space=pltpu.VMEM)
    return pl.pallas_call(
        mixer_kernel,
        out_shape=jax.ShapeDtypeStruct((rows, ow), bf16),
        in_specs=[anywhere] * 5 + [vmem] * 3,
        out_specs=vmem,
        scratch_shapes=[
            pltpu.VMEM((total, depth), bf16),
            pltpu.VMEM((total, depth), bf16),
            pltpu.VMEM((total, channels), bf16),
            pltpu.VMEM((LAYERS, depth, 3 * wide), bf16),
            pltpu.VMEM((LAYERS, channels, owide), bf16),
            pltpu.VMEM((total, 3 * wide), f32),
            pltpu.VMEM((8, wide), f32),
            pltpu.VMEM((4, rows, owide), bf16),
            pltpu.VMEM((rows, ow), bf16),
            pltpu.VMEM((8, depth), f32),
            pltpu.VMEM((8, ow), f32),
            pltpu.VMEM((lanes, 8, rows), f32),
            dma((1 + 2 * LAYERS,)),
            dma((3, 3 * LAYERS)),
            dma((3, 3 * LAYERS)),
            dma((2, CHUNKS, 7)),
            dma((2, CHUNKS, 7)),
            dma((16,)),
            dma((20,)),
        ],
        compiler_params=pltpu.CompilerParams(has_side_effects=True, vmem_limit_bytes=VMEM_BYTES),
    )(tokens, proj_b, proj_c, proj_x, proj_out, conv_taps, ln_gain, ln_bias)


def solution(mesh):
    specs = dict(
        mesh=mesh,
        in_specs=(
            P(("grp", "sp"), "tp"),
            P(None, "sp", "tp"),
            P(None, "sp", "tp"),
            P(None, "sp", "tp"),
            P(None, "sp", "tp"),
            P(None, None, "tp"),
            P(None, "tp"),
            P(None, "tp"),
        ),
        out_specs=P(("grp", "sp"), "tp"),
        check_vma=False,
    )
    if (mesh.shape["grp"], mesh.shape["sp"], mesh.shape["tp"]) == (2, 4, 4):
        return jax.shard_map(mixer, **specs)
    return jax.shard_map(local, **specs)
```

profile of v0, /device:TPU:0, one launch (start us, length us, event | category | flops | bytes accessed | tf_op | source)
XLA Modules:
  0.0 349.6 jit_solution(15706388883192640339)
XLA Ops:
  0.0 1.3 copy.9.conv_taps
  1.3 346.2 %shard_map.82 = bf16[384,1024]{1,0:T(8,128)(2,1)} custom-call(bf16[384,1024]{1,0:T(8,128)(2,1)} %tokens.1, bf16[2,1024,512]{2,1,0:T(8,128)(2,1)} %proj_b.1, bf16[2,1024,512]{2,1,0:T(8,128)(2,1)} %proj_c.1, bf16[2,1024,512]{2,1,0:T(8,128)(2,1)} %proj_x.1, bf16[2,512,1024]{2,1,0:T(8,128)(2,1)} %proj_out.1, f32[2,3,512]{2,1,0:T(4,128)} %copy.9.conv_taps, ...), custom_call_target="tpu_custom_call" | custom-call | tf_op jit(solution)/shard_map/pallas_call | solution.py:515
  347.5 2.1 copy.11
where the time goes:
time: 350 us
  Pallas kernels  346 us (99%)
    pallas_call x1, Pallas kernels, mixer(): pl.pallas_call(mixer_kernel, out_shape=jax.ShapeDtypeStruct((rows, ow), b...  346 us

commit v1 on v0

--- a/solution.py
+++ b/solution.py
@@ -123,7 +123,7 @@
 
 def mixer_kernel(
     tokens, proj_b, proj_c, proj_x, proj_out, conv_taps, ln_gain, ln_bias, out,
-    hidden, raw, branch, w_in, w_out, acc, carry, stage, final, scales, own_scales, stats,
+    hidden, raw, branch, w_in, w_out, acc, carry, stage, final, scales, own_scales, stats, ones, means,
     local_sem, w_send, w_recv, ag_send, ag_recv, small_send, small_recv,
 ):
     f32, bf16 = jnp.float32, jnp.bfloat16
@@ -134,67 +134,93 @@
     rows, ow = tokens.shape
     kin, kout = proj_b.shape[1], proj_out.shape[1]
     wide, owide = proj_b.shape[2] // parts, ow // parts
-    reach = conv_taps.shape[1] - 1
+    reach = conv_taps.shape[0] - 1
     part_rows = HALO + 2 * rows
     chunk_rows = parts * part_rows // CHUNKS
     half = s // 2
     base, end, mid = 2 * half, 3 * half, 1 + half
     other, far = 2 - half, 3 - 3 * half
     projections = (proj_b, proj_c, proj_x)
-    kc = kin // 2
+    sub = wide // 2
+    pieces_in, pieces = (0, 1), 3
 
     def copy(src, dst, send, recv, device):
         return pltpu.make_async_remote_copy(src, dst, send, recv, device_id=device, device_id_type=MESH)
 
     def piece(layer, block, k):
-        if k == 2:
-            return w_out.at[layer, pl.ds(multiple(block * kout, kout), kout), :]
-        return w_in.at[layer, pl.ds(multiple(block * kin + k * kc, kc), kc), :]
+        if k in pieces_in:
+            return w_in.at[layer, k, pl.ds(multiple(block * kin, kin), kin), :]
+        return w_out.at[layer, pl.ds(multiple(block * kout, kout), kout), :]
+
+    def piece_parts(layer, k):
+        if k in pieces_in:
+            columns = pl.ds(multiple(g * wide + k * sub, sub), sub)
+            rows_there = pl.ds(multiple(s * kin, kin), kin)
+            for j, w in enumerate(projections):
+                yield w.at[layer, :, columns], w_in.at[layer, k, rows_there, pl.ds(j * sub, sub)]
+        else:
+            columns = pl.ds(multiple(g * owide, owide), owide)
+            yield proj_out.at[layer, :, columns], piece(layer, s, k)
 
     def send_own(layer, k, device, row):
-        sems = (w_send.at[row, layer * 3 + k], w_recv.at[row, layer * 3 + k])
-        if k == 2:
-            src = proj_out.at[layer, :, pl.ds(multiple(g * owide, owide), owide)]
-            copy(src, piece(layer, s, k), *sems, device).start()
-        else:
-            for j, w in enumerate(projections):
-                src = w.at[layer, pl.ds(k * kc, kc), pl.ds(multiple(g * wide, wide), wide)]
-                dst = w_in.at[layer, pl.ds(multiple(s * kin + k * kc, kc), kc), pl.ds(j * wide, wide)]
-                copy(src, dst, *sems, device).start()
+        sems = (w_send.at[row, layer * pieces + k], w_recv.at[row, layer * pieces + k])
+        for src, dst in piece_parts(layer, k):
+            copy(src, dst, *sems, device).start()
 
     def w_wait(layer, k, row, block, sent=False):
         ref = piece(layer, block, k)
-        c_ = copy(ref, ref, w_send.at[row, layer * 3 + k], w_recv.at[row, layer * 3 + k], (g, s, t))
-        c_.wait_send() if sent else c_.wait_recv()
+        done = copy(ref, ref, w_send.at[row, layer * pieces + k], w_recv.at[row, layer * pieces + k], (g, s, t))
+        done.wait_send() if sent else done.wait_recv()
 
     def relay(layer, k):
         w_wait(layer, k, 0, end)
         ref = piece(layer, end, k)
-        copy(ref, ref, w_send.at[2, layer * 3 + k], w_recv.at[2, layer * 3 + k], (g, other, t)).start()
-
-    pieces = [(layer, k) for layer in range(LAYERS) for k in range(3)]
+        sems = (w_send.at[2, layer * pieces + k], w_recv.at[2, layer * pieces + k])
+        copy(ref, ref, *sems, (g, other, t)).start()
+
+    order = [(layer, k) for layer in range(LAYERS) for k in range(pieces)]
 
     def token_rows(index):
         return pl.ds(multiple(g * part_rows + HALO + index * rows, 16), rows)
 
-    own_columns = pl.ds(multiple(t * ow + g * owide, owide), owide)
-
-    def final_half(gg):
+    def final_part(gg):
         return final.at[:, pl.ds(multiple(gg * owide, owide), owide)]
+
+    def final_arrived(gg):
+        ref = final_part(gg)
+        copy(ref, ref, small_send.at[2], small_recv.at[8 + gg], (g, s, t)).wait_recv()
+
+    barrier = pltpu.get_barrier_semaphore()
+
+    def greet(devices):
+        for device in devices:
+            pl.semaphore_signal(barrier, inc=1, device_id=device, device_id_type=MESH)
+        pl.semaphore_wait(barrier, len(devices))
+
+    lane_peers = [(g, s, (t + k) % lanes) for k in range(1, lanes)]
+
+    def end_slab(j):
+        start = multiple(g * part_rows + HALO + (end - base) * rows + j * (rows // 2), 16)
+        return hidden.at[pl.ds(start, rows // 2), pl.ds(multiple(t * ow, ow), ow)]
+
+    def end_tokens(j):
+        return copy(
+            tokens.at[pl.ds(j * (rows // 2), rows // 2), :], end_slab(j),
+            small_send.at[3 * j], small_recv.at[3 * j], (g, mid, t),
+        )
 
     @pl.when(s == end)
     def _():
-        slab = hidden.at[token_rows(end - base), pl.ds(multiple(t * ow, ow), ow)]
-        copy(tokens, slab, small_send.at[0], small_recv.at[0], (g, mid, t)).start()
-        for i, (layer, k) in enumerate(pieces):
-            if i >= 2:
-                w_wait(*pieces[i - 2], 0, s, sent=True)
+        greet(lane_peers + [(gg, mid, t) for gg in range(parts)])
+        for j in range(2):
+            end_tokens(j).start()
+        for j in range(2):
+            end_tokens(j).wait_send()
+        for layer, k in order:
             send_own(layer, k, (g, mid, t), 0)
-        for layer, k in pieces[-2:]:
             w_wait(layer, k, 0, s, sent=True)
-        copy(tokens, slab, small_send.at[0], small_recv.at[0], (g, mid, t)).wait_send()
         for gg in range(parts):
-            copy(final_half(gg), final_half(gg), small_send.at[2], small_recv.at[8 + gg], (g, s, t)).wait_recv()
+            final_arrived(gg)
 
     @pl.when(s == mid)
     def _():
@@ -205,22 +231,13 @@
         diagonal = (1 - g, mid, 2 * (1 - x) + c)
         me = (g, mid, t)
 
-        for k in range(2):
-            send_own(0, k, there, 1)
+        greet(lane_peers + [(1 - g, mid, t), there] + [(gg, end, t) for gg in range(parts)])
+        send_own(0, 0, there, 1)
         mine = hidden.at[token_rows(mid - base), pl.ds(multiple(t * ow, ow), ow)]
         pltpu.make_async_copy(tokens, mine, local_sem.at[0]).start()
-        for layer in range(LAYERS):
-            for j, w in enumerate(projections):
-                pltpu.make_async_copy(
-                    w.at[layer, :, pl.ds(multiple(g * wide, wide), wide)],
-                    w_in.at[layer, pl.ds(multiple(s * kin, kin), kin), pl.ds(j * wide, wide)],
-                    local_sem.at[1 + layer],
-                ).start()
-            pltpu.make_async_copy(
-                proj_out.at[layer, :, pl.ds(multiple(g * owide, owide), owide)],
-                piece(layer, s, 2),
-                local_sem.at[1 + LAYERS + layer],
-            ).start()
+        for layer, k in order:
+            for src, dst in piece_parts(layer, k):
+                pltpu.make_async_copy(src, dst, local_sem.at[1 + layer * pieces + k]).start()
 
         edge = hidden.at[pl.ds(multiple(g * part_rows, 16), HALO), pl.ds(multiple(t * ow, ow), ow)]
         edge_copy = copy(tokens.at[pl.ds(rows - HALO, HALO), :], edge, small_send.at[1], small_recv.at[1], there)
@@ -239,7 +256,7 @@
                 small_send.at[4 + k], small_recv.at[4 + k], (g, s, (t + k) % lanes),
             ).start()
 
-        def gather(buffer, region, family, produce, consume, unroll=False):
+        def gather(buffer, region, count, family, produce, consume, ahead, unroll=False):
             def at(device, i):
                 return buffer.at[region(device[0], device[2], i)]
 
@@ -251,142 +268,174 @@
                 transfer(me, i, role, 0, me).wait_recv()
 
             def send(i):
+                produce(i)
                 transfer(me, i, 0, 0, up).start()
                 transfer(me, i, 1, 1, vp).start()
                 transfer(me, i, 3, 2, pp).start()
 
-            def step(i):
+            def pass_on(i):
                 arrived(i, 0)
                 transfer(up, i, 2, 4, vp).start()
                 transfer(up, i, 4, 3, pp).start()
                 arrived(i, 1)
                 transfer(vp, i, 5, 5, pp).start()
+
+            def finish(i):
                 arrived(i, 2)
                 transfer(diagonal, i, 6, 6, pp).start()
                 for role in range(3, 7):
                     arrived(i, role)
                 consume(i)
 
-            produce(0)
-            send(0)
+            def sent(i):
+                for kind in range(7):
+                    transfer(me, i, 0, kind, me).wait_send()
+
+            for i in range(ahead):
+                send(i)
             if unroll:
-                for i in range(CHUNKS):
-                    if i + 1 < CHUNKS:
-                        produce(i + 1)
-                        send(i + 1)
-                    step(i)
+                for i in range(count + 1):
+                    if i + ahead < count:
+                        send(i + ahead)
+                    if i < count:
+                        pass_on(i)
+                    if i:
+                        finish(i - 1)
+                for i in range(count):
+                    sent(i)
             else:
-                @pl.loop(0, CHUNKS)
+                @pl.loop(0, count + 1)
                 def _(i):
-                    @pl.when(i + 1 < CHUNKS)
+                    @pl.when(i + ahead < count)
                     def _():
-                        produce(i + 1)
-                        send(i + 1)
-
-                    step(i)
+                        send(i + ahead)
+
+                    @pl.when(i < count)
+                    def _():
+                        pass_on(i)
+
+                    @pl.when(i > 0)
+                    def _():
+                        finish(i - 1)
+
+                @pl.loop(0, count)
+                def _(i):
+                    sent(i)
+
+        def row_chunk(i):
+            return pl.ds(multiple(i * chunk_rows, 16), chunk_rows)
+
+        def nothing(i):
+            pass
+
+        first_half = rows // 2
+        token_starts = (
+            HALO + (mid - base) * rows,
+            HALO + (mid - base) * rows + first_half,
+            0,
+            HALO + (end - base) * rows,
+            HALO + (end - base) * rows + first_half,
+        )
+
+        def token_region(gg, tt, i):
+            length = HALO if i == 2 else first_half
+            return (
+                pl.ds(multiple(gg * part_rows + token_starts[i], 16), length),
+                pl.ds(multiple(tt * ow, ow), ow),
+            )
+
+        def token_ready(i):
+            if i == 0:
+                pltpu.make_async_copy(tokens, mine, local_sem.at[0]).wait()
+            if i == 2:
+                @pl.when(half == 1)
+                def _():
+                    edge_copy.wait_recv()
+            if i > 2:
+                slab = end_slab(i - 3)
+                copy(slab, slab, small_send.at[3 * (i - 3)], small_recv.at[3 * (i - 3)], me).wait_recv()
+
+        def token_hook(i):
+            if i == 0:
+                send_own(0, 1, there, 1)
+            if i == 3:
+                relay(0, 0)
+            if i == 4:
+                relay(0, 1)
+
+        gather(hidden, token_region, 5, 0, token_ready, token_hook, 2, unroll=True)
+
+        def accumulate(layer, k, start, depth, i, first=False):
+            at_rows = row_chunk(i)
+            term = jnp.dot(
+                hidden[at_rows, pl.ds(multiple(start, kin), depth)],
+                w_in[layer, k, pl.ds(multiple(start, kin), depth), :],
+                preferred_element_type=f32,
+            )
+            acc[k, at_rows, :] = term if first else acc[k, at_rows, :] + term
+
+        def wait_near(layer, k):
+            ref = piece(layer, s, k)
+            pltpu.make_async_copy(ref, ref, local_sem.at[1 + layer * pieces + k]).wait()
+
+        def near_in(layer, k, i):
+            accumulate(layer, k, base * kin, 2 * kin, i, first=True)
+
+        def far_in(layer, k):
+            for row, block in ((1, other), (2, far)):
+                w_wait(layer, k, row, block)
 
             @pl.loop(0, CHUNKS)
             def _(i):
-                for kind in range(7):
-                    transfer(me, i, 0, kind, me).wait_send()
-
-        def row_chunk(i):
-            return pl.ds(multiple(i * chunk_rows, 16), chunk_rows)
-
-        def nothing(i):
-            pass
-
-        def token_hook(i):
-            if i in (1, 2):
-                relay(0, i - 1)
-            if i == 2:
-                send_own(0, 2, there, 1)
-
-        pltpu.make_async_copy(tokens, mine, local_sem.at[0]).wait()
-        theirs = hidden.at[token_rows(end - base), pl.ds(multiple(t * ow, ow), ow)]
-        copy(theirs, theirs, small_send.at[0], small_recv.at[0], me).wait_recv()
-
-        @pl.when(half == 1)
-        def _():
-            edge_copy.wait_recv()
-
-        qw = ow // CHUNKS
-        gather(
-            hidden,
-            lambda gg, tt, i: (
-                pl.ds(multiple(gg * part_rows, 16), part_rows),
-                pl.ds(multiple(tt * ow + i * qw, qw), qw),
-            ),
-            0, nothing, token_hook, unroll=True,
-        )
-
-        def accumulate(layer, start, depth, i, first=False):
-            at_rows = row_chunk(i)
-            term = jnp.dot(
-                hidden[at_rows, pl.ds(multiple(start, kc), depth)],
-                w_in[layer, pl.ds(multiple(start, kc), depth), :],
-                preferred_element_type=f32,
-            )
-            acc[at_rows, :] = term if first else acc[at_rows, :] + term
-
-        def wait_near_in(layer):
-            ref = w_in.at[layer, pl.ds(multiple(s * kin, kin), kin), :]
-            pltpu.make_async_copy(ref, ref, local_sem.at[1 + layer]).wait()
-
-        def near_in(layer, i):
-            accumulate(layer, base * kin, 2 * kin, i, first=True)
-
-        def far_in(layer):
-            for row, block in ((1, other), (2, far)):
-                for k in range(2):
-                    w_wait(layer, k, row, block)
-
-                    @pl.loop(0, CHUNKS)
-                    def _(i):
-                        accumulate(layer, block * kin + k * kc, kc, i)
+                accumulate(layer, k, 2 * (1 - half) * kin, 2 * kin, i)
 
         tr = tile_rows(chunk_rows, 96)
 
-        def gate(layer, i):
+        def branch_columns(gg, tt, k):
+            return pl.ds(multiple(tt * parts * wide + gg * wide + k * sub, sub), sub)
+
+        def gate(layer, k, i):
             taps = [
-                conv_taps[layer, k : k + 1, pl.ds(multiple(g * wide, wide), wide)] for k in range(reach + 1)
+                conv_taps[n, layer : layer + 1, pl.ds(multiple(g * wide + k * sub, sub), sub)] for n in range(reach + 1)
             ]
-            row_of = lax.broadcasted_iota(jnp.int32, (tr, wide), 0)
+            row_of = lax.broadcasted_iota(jnp.int32, (tr, sub), 0)
 
             @pl.loop(0, chunk_rows // tr)
             def _(q):
                 start = multiple(i * chunk_rows + q * tr, 16)
                 position = start % part_rows
-                sums = acc[pl.ds(start, tr), :].astype(bf16).astype(f32)
-                out_gate, in_gate, values = (sums[:, j * wide : (j + 1) * wide] for j in range(3))
+                sums = acc[k, pl.ds(start, tr), :].astype(bf16).astype(f32)
+                out_gate, in_gate, values = (sums[:, j * sub : (j + 1) * sub] for j in range(3))
                 gated = in_gate * values
                 gated = jnp.where(row_of < HALO * (1 - half) - position, 0.0, gated)
                 before = jnp.where(position == 0, 0.0, carry[...])
                 conv = jnp.zeros_like(gated)
-                for k in range(reach + 1):
-                    shift = reach - k
+                for n in range(reach + 1):
+                    shift = reach - n
                     moved = gated
                     if shift:
                         moved = pltpu.roll(gated, shift, 0)
                         for j in range(shift):
                             moved = jnp.where(row_of == j, before[8 - shift + j : 8 - shift + j + 1, :], moved)
-                    conv = conv + taps[k] * moved
+                    conv = conv + taps[n] * moved
                 carry[...] = gated[tr - 8 :, :]
-                branch[pl.ds(start, tr), pl.ds(multiple(t * parts * wide + g * wide, wide), wide)] = (
-                    out_gate * conv
-                ).astype(bf16)
-
-        def branch_region(gg, tt, i):
-            return row_chunk(i), pl.ds(multiple(tt * parts * wide + gg * wide, wide), wide)
+                branch[pl.ds(start, tr), branch_columns(g, t, k)] = (out_gate * conv).astype(bf16)
+
+        def branches(layer, k, consume):
+            gather(
+                branch, lambda gg, tt, i: (row_chunk(i), branch_columns(gg, tt, k)),
+                CHUNKS, 1 + k, lambda i: gate(layer, k, i), consume, 2,
+            )
 
         def sum_region(gg, tt, i):
             return row_chunk(i), pl.ds(multiple(tt * ow + gg * owide, owide), owide)
 
         def wait_out(layer):
-            ref = piece(layer, s, 2)
-            pltpu.make_async_copy(ref, ref, local_sem.at[1 + LAYERS + layer]).wait()
+            wait_near(layer, 2)
             for row, block in ((1, other), (2, far)):
                 w_wait(layer, 2, row, block)
+
+        own_columns = pl.ds(multiple(t * ow + g * owide, owide), owide)
 
         def mix(layer, at_rows):
             mixed = jnp.dot(branch[at_rows, :], w_out[layer], preferred_element_type=f32)
@@ -396,54 +445,83 @@
         def produce_sum(i):
             raw[row_chunk(i), own_columns] = mix(0, row_chunk(i))
 
+        strips = [slice(n, n + 128) for n in range(0, hidden.shape[1], 128)]
+        ones[...] = jnp.ones_like(ones)
+
         def normalise(i):
-            @pl.loop(0, chunk_rows // 16)
+            means[...] = jnp.dot(raw[row_chunk(i), :], ones[...], preferred_element_type=f32) / ones.shape[0]
+
+            @pl.loop(0, chunk_rows // tr)
             def _(q):
-                at_rows = pl.ds(multiple(i * chunk_rows + q * 16, 16), 16)
-                summed = raw[at_rows, :].astype(f32)
-                mean = jnp.mean(summed, axis=1, keepdims=True)
-                centered = summed - mean
-                variance = jnp.mean(centered * centered, axis=1, keepdims=True)
-                hidden[at_rows, :] = (
-                    centered * lax.rsqrt(variance + norm_eps) * scales[0:1, :] + scales[1:2, :]
-                ).astype(bf16)
+                there_rows = pl.ds(multiple(i * chunk_rows + q * tr, 16), tr)
+                here_rows = pl.ds(multiple(q * tr, 16), tr)
+                mean = means[here_rows, :]
+                total = jnp.zeros_like(mean)
+                for strip in strips:
+                    centered = raw[there_rows, strip].astype(f32) - mean
+                    total = total + centered * centered
+                scale = lax.rsqrt(jnp.sum(total, axis=1, keepdims=True) / ones.shape[0] + norm_eps)
+                scale = jnp.broadcast_to(scale, mean.shape)
+                for strip in strips:
+                    centered = raw[there_rows, strip].astype(f32) - mean
+                    hidden[there_rows, strip] = (
+                        centered * scale * scales[0:1, strip] + scales[1:2, strip]
+                    ).astype(bf16)
+
+        def send_pair(layer, k):
+            send_own(layer, k, there, 1)
+            relay(layer, k)
 
         def consume_sum(i):
             normalise(i)
-            near_in(1, i)
-
-        wait_near_in(0)
+            near_in(1, 0, i)
+
+            @pl.when(i == 0)
+            def _():
+                send_pair(1, 1)
+
+            near_in(1, 1, i)
+
+        def first_branches(i):
+            near_in(0, 1, i)
+
+            @pl.when(i == CHUNKS - 1)
+            def _():
+                send_pair(0, 2)
+
+        for k in pieces_in:
+            wait_near(0, k)
 
         @pl.loop(0, CHUNKS)
         def _(i):
-            near_in(0, i)
-
-        relay(0, 2)
-        for k in range(2):
-            send_own(1, k, there, 1)
-        far_in(0)
-        gather(branch, branch_region, 1, lambda i: gate(0, i), nothing)
-        for k in range(2):
-            relay(1, k)
-        send_own(1, 2, there, 1)
+            near_in(0, 0, i)
+
+        far_in(0, 0)
+        branches(0, 0, first_branches)
+        far_in(0, 1)
+        branches(0, 1, nothing)
+        send_pair(1, 0)
         for k in range(1, lanes):
             copy(
                 own_scales, scales.at[:, pl.ds(multiple(((t + lanes - k) % lanes) * ow, ow), ow)],
                 small_send.at[4 + k], small_recv.at[4 + k], me,
             ).wait()
         wait_out(0)
-        wait_near_in(1)
-        gather(raw, sum_region, 0, produce_sum, consume_sum)
-        relay(1, 2)
-        far_in(1)
-        gather(branch, branch_region, 1, lambda i: gate(1, i), nothing)
+        for k in pieces_in:
+            wait_near(1, k)
+        gather(raw, sum_region, CHUNKS, 0, produce_sum, consume_sum, 1)
+        far_in(1, 0)
+        send_pair(1, 2)
+        branches(1, 0, nothing)
+        far_in(1, 1)
+        branches(1, 1, nothing)
         wait_out(1)
 
         def result_copy(j):
             p = (g + 1 + j // 2) % 2
             to = end + (j % 2) * (mid - end)
             return p, to, copy(
-                stage.at[j], final_half(g), small_send.at[12 + j], small_recv.at[8 + g], (p, to, t)
+                stage.at[j], final_part(g), small_send.at[12 + j], small_recv.at[8 + g], (p, to, t)
             )
 
         @pl.loop(0, 4)
@@ -458,7 +536,7 @@
         final[:, pl.ds(multiple(g * owide, owide), owide)] = stage[3]
         for j in range(3):
             result_copy(j)[2].wait_send()
-        for layer, k in pieces:
+        for layer, k in order:
             w_wait(layer, k, 1, s, sent=True)
             w_wait(layer, k, 2, end, sent=True)
 
@@ -466,7 +544,7 @@
         def _():
             edge_copy.wait_send()
 
-        copy(final_half(1 - g), final_half(1 - g), small_send.at[2], small_recv.at[8 + 1 - g], me).wait_recv()
+        final_arrived(1 - g)
 
     lane = lax.broadcasted_iota(jnp.int32, (128, 128), 1)
     line = lax.broadcasted_iota(jnp.int32, (128, 128), 0)
@@ -521,25 +599,29 @@
             pltpu.VMEM((total, depth), bf16),
             pltpu.VMEM((total, depth), bf16),
             pltpu.VMEM((total, channels), bf16),
-            pltpu.VMEM((LAYERS, depth, 3 * wide), bf16),
+            pltpu.VMEM((LAYERS, 2, depth, 3 * wide // 2), bf16),
             pltpu.VMEM((LAYERS, channels, owide), bf16),
-            pltpu.VMEM((total, 3 * wide), f32),
-            pltpu.VMEM((8, wide), f32),
+            pltpu.VMEM((2, total, 3 * wide // 2), f32),
+            pltpu.VMEM((8, wide // 2), f32),
             pltpu.VMEM((4, rows, owide), bf16),
             pltpu.VMEM((rows, ow), bf16),
             pltpu.VMEM((8, depth), f32),
             pltpu.VMEM((8, ow), f32),
             pltpu.VMEM((lanes, 8, rows), f32),
-            dma((1 + 2 * LAYERS,)),
+            pltpu.VMEM((depth, 128), bf16),
+            pltpu.VMEM((total // CHUNKS, 128), f32),
+            dma((1 + 3 * LAYERS,)),
             dma((3, 3 * LAYERS)),
             dma((3, 3 * LAYERS)),
-            dma((2, CHUNKS, 7)),
-            dma((2, CHUNKS, 7)),
-            dma((16,)),
+            dma((3, 5, 7)),
+            dma((3, 5, 7)),
+            dma((20,)),
             dma((20,)),
         ],
-        compiler_params=pltpu.CompilerParams(has_side_effects=True, vmem_limit_bytes=VMEM_BYTES),
-    )(tokens, proj_b, proj_c, proj_x, proj_out, conv_taps, ln_gain, ln_bias)
+        compiler_params=pltpu.CompilerParams(
+            has_side_effects=True, collective_id=0, vmem_limit_bytes=VMEM_BYTES
+        ),
+    )(tokens, proj_b, proj_c, proj_x, proj_out, conv_taps.transpose(1, 0, 2), ln_gain, ln_bias)
 
 
 def solution(mesh):

time: 350 us -> 273 us (0.78)
  Pallas kernels: 346 us -> 271 us
    pallas_call x1, Pallas kernels: 346 us -> 271 us  [mixer(): pl.pallas_call(mixer_kernel, out_shape=jax.ShapeDtypeStruct((rows, ow), b...]
where the time goes in v1:
time: 273 us
  Pallas kernels  271 us (99%)
    pallas_call x1, Pallas kernels, mixer(): pl.pallas_call(mixer_kernel, out_shape=jax.ShapeDtypeStruct((rows, ow), b...  271 us

profile of v1, /device:TPU:0, one launch (start us, length us, event | category | flops | bytes accessed | tf_op | source)
XLA Modules:
  0.0 272.9 jit_solution(6070402203664235812)
XLA Ops:
  0.0 270.8 %shard_map.82 = bf16[384,1024]{1,0:T(8,128)(2,1)} custom-call(bf16[384,1024]{1,0:T(8,128)(2,1)} %tokens.1, bf16[2,1024,512]{2,1,0:T(8,128)(2,1)} %proj_b.1, bf16[2,1024,512]{2,1,0:T(8,128)(2,1)} %proj_c.1, bf16[2,1024,512]{2,1,0:T(8,128)(2,1)} %proj_x.1, bf16[2,512,1024]{2,1,0:T(8,128)(2,1)} %proj_out.1, f32[3,2,512]{2,1,0:T(2,128)} %bitcast.1, ...), custom_call_target="tpu_custom_call" | custom-call | tf_op jit(solution)/shard_map/pallas_call | solution.py:593
  270.8 2.1 copy.10

commit v2 on v1

--- a/solution.py
+++ b/solution.py
@@ -108,7 +108,14 @@
 
 
 MESH = pl.DeviceIdType.MESH
-CHUNKS = 4
+BRANCH_CHUNKS = 5
+SUM_CHUNKS = 5
+BRANCH_AHEAD = 1
+TOKEN_AHEAD = 1
+TOKEN_HOOK = 2
+SUM_AHEAD = 1
+BRANCH_VIA_END = 1
+SUM_VIA_END = 1
 HALO = 32
 VMEM_BYTES = 63 * 2**20
 
@@ -136,12 +143,12 @@
     wide, owide = proj_b.shape[2] // parts, ow // parts
     reach = conv_taps.shape[0] - 1
     part_rows = HALO + 2 * rows
-    chunk_rows = parts * part_rows // CHUNKS
+    total = parts * part_rows
     half = s // 2
     base, end, mid = 2 * half, 3 * half, 1 + half
     other, far = 2 - half, 3 - 3 * half
     projections = (proj_b, proj_c, proj_x)
-    sub = wide // 2
+    kc = kin // 2
     pieces_in, pieces = (0, 1), 3
 
     def copy(src, dst, send, recv, device):
@@ -149,15 +156,15 @@
 
     def piece(layer, block, k):
         if k in pieces_in:
-            return w_in.at[layer, k, pl.ds(multiple(block * kin, kin), kin), :]
+            return w_in.at[layer, pl.ds(multiple(block * kin + k * kc, kc), kc), :]
         return w_out.at[layer, pl.ds(multiple(block * kout, kout), kout), :]
 
     def piece_parts(layer, k):
         if k in pieces_in:
-            columns = pl.ds(multiple(g * wide + k * sub, sub), sub)
-            rows_there = pl.ds(multiple(s * kin, kin), kin)
+            columns = pl.ds(multiple(g * wide, wide), wide)
+            rows_there = pl.ds(multiple(s * kin + k * kc, kc), kc)
             for j, w in enumerate(projections):
-                yield w.at[layer, :, columns], w_in.at[layer, k, rows_there, pl.ds(j * sub, sub)]
+                yield w.at[layer, pl.ds(k * kc, kc), columns], w_in.at[layer, rows_there, pl.ds(j * wide, wide)]
         else:
             columns = pl.ds(multiple(g * owide, owide), owide)
             yield proj_out.at[layer, :, columns], piece(layer, s, k)
@@ -190,6 +197,24 @@
         ref = final_part(gg)
         copy(ref, ref, small_send.at[2], small_recv.at[8 + gg], (g, s, t)).wait_recv()
 
+    yu, xu = g + c * (1 - 2 * g), x + (1 - c) * (1 - 2 * x)
+    yv, xv = g + (1 - c) * (1 - 2 * g), x + c * (1 - 2 * x)
+    up, vp, pp = (yu, s, 2 * xu + c), (yv, s, 2 * xv + c), (g, s, 2 * x + 1 - c)
+    diagonal = (1 - g, s, 2 * (1 - x) + c)
+    me = (g, s, t)
+
+    def row_chunk(i, count):
+        return pl.ds(multiple(i * (total // count), 16), total // count)
+
+    def branch_columns(gg, tt):
+        return pl.ds(multiple(tt * parts * wide + gg * wide, wide), wide)
+
+    def branch_region(gg, tt, i):
+        return row_chunk(i, BRANCH_CHUNKS), branch_columns(gg, tt)
+
+    def sum_region(gg, tt, i):
+        return row_chunk(i, SUM_CHUNKS), pl.ds(multiple(tt * ow + gg * owide, owide), owide)
+
     barrier = pltpu.get_barrier_semaphore()
 
     def greet(devices):
@@ -211,28 +236,51 @@
 
     @pl.when(s == end)
     def _():
-        greet(lane_peers + [(gg, mid, t) for gg in range(parts)])
-        for j in range(2):
-            end_tokens(j).start()
-        for j in range(2):
-            end_tokens(j).wait_send()
+        greet(lane_peers + [(1 - g, end, t)] + [(gg, mid, t) for gg in range(parts)])
+
+        def send_tokens():
+            for j in range(2):
+                end_tokens(j).start()
+            for j in range(2):
+                end_tokens(j).wait_send()
+
+        send_tokens()
         for layer, k in order:
             send_own(layer, k, (g, mid, t), 0)
             w_wait(layer, k, 0, s, sent=True)
+
+        def pass_through(buffer, region, count, family, via):
+            def transfer(owner, i, role, kind, device):
+                ref = buffer.at[region(owner[0], owner[2], i)]
+                return copy(ref, ref, ag_send.at[family, i, kind], ag_recv.at[family, i, role], device)
+
+            through_end = range(count - via, count)
+            for i in through_end:
+                transfer(me, i, 3, 0, me).wait_recv()
+                transfer(me, i, 0, 0, up).start()
+                transfer(me, i, 1, 1, vp).start()
+            for i in through_end:
+                for role, owner in enumerate((up, vp, diagonal)):
+                    transfer(me, i, role, 0, me).wait_recv()
+                    if role == 0:
+                        transfer(up, i, 2, 4, vp).start()
+                    transfer(owner, i, role, (2, 3, 5)[role], (g, mid, t)).start()
+            for i in through_end:
+                for kind in range(6):
+                    transfer(me, i, 0, kind, me).wait_send()
+
+        pass_through(raw, sum_region, SUM_CHUNKS, 0, SUM_VIA_END)
+        pass_through(branch, branch_region, BRANCH_CHUNKS, 2, BRANCH_VIA_END)
         for gg in range(parts):
             final_arrived(gg)
 
     @pl.when(s == mid)
     def _():
         there = (g, other, t)
-        yu, xu = g + c * (1 - 2 * g), x + (1 - c) * (1 - 2 * x)
-        yv, xv = g + (1 - c) * (1 - 2 * g), x + c * (1 - 2 * x)
-        up, vp, pp = (yu, mid, 2 * xu + c), (yv, mid, 2 * xv + c), (g, mid, 2 * x + 1 - c)
-        diagonal = (1 - g, mid, 2 * (1 - x) + c)
-        me = (g, mid, t)
 
         greet(lane_peers + [(1 - g, mid, t), there] + [(gg, end, t) for gg in range(parts)])
-        send_own(0, 0, there, 1)
+        for k in pieces_in:
+            send_own(0, k, there, 1)
         mine = hidden.at[token_rows(mid - base), pl.ds(multiple(t * ow, ow), ow)]
         pltpu.make_async_copy(tokens, mine, local_sem.at[0]).start()
         for layer, k in order:
@@ -256,7 +304,7 @@
                 small_send.at[4 + k], small_recv.at[4 + k], (g, s, (t + k) % lanes),
             ).start()
 
-        def gather(buffer, region, count, family, produce, consume, ahead, unroll=False):
+        def gather(buffer, region, count, family, produce, consume, ahead, unroll=False, via=0, between=None):
             def at(device, i):
                 return buffer.at[region(device[0], device[2], i)]
 
@@ -287,10 +335,16 @@
                     arrived(i, role)
                 consume(i)
 
-            def sent(i):
-                for kind in range(7):
+            def sent(i, kinds):
+                for kind in kinds:
                     transfer(me, i, 0, kind, me).wait_send()
 
+            through_end = range(count - via, count)
+            for i in through_end:
+                produce(i)
+                transfer(me, i, 3, 0, (g, end, t)).start()
+                transfer(me, i, 3, 2, pp).start()
+            count = count - via
             for i in range(ahead):
                 send(i)
             if unroll:
@@ -299,10 +353,10 @@
                         send(i + ahead)
                     if i < count:
                         pass_on(i)
+                    if between:
+                        between(i)
                     if i:
                         finish(i - 1)
-                for i in range(count):
-                    sent(i)
             else:
                 @pl.loop(0, count + 1)
                 def _(i):
@@ -318,12 +372,20 @@
                     def _():
                         finish(i - 1)
 
+            for i in through_end:
+                arrived(i, 0)
+                transfer(up, i, 4, 3, pp).start()
+                arrived(i, 1)
+                transfer(vp, i, 5, 5, pp).start()
+                finish(i)
+                sent(i, (0, 2, 3, 5, 6))
+            if unroll:
+                for i in range(count):
+                    sent(i, range(7))
+            else:
                 @pl.loop(0, count)
                 def _(i):
-                    sent(i)
-
-        def row_chunk(i):
-            return pl.ds(multiple(i * chunk_rows, 16), chunk_rows)
+                    sent(i, range(7))
 
         def nothing(i):
             pass
@@ -356,56 +418,59 @@
                 copy(slab, slab, small_send.at[3 * (i - 3)], small_recv.at[3 * (i - 3)], me).wait_recv()
 
         def token_hook(i):
-            if i == 0:
-                send_own(0, 1, there, 1)
-            if i == 3:
+            if i == TOKEN_HOOK:
                 relay(0, 0)
             if i == 4:
                 relay(0, 1)
 
-        gather(hidden, token_region, 5, 0, token_ready, token_hook, 2, unroll=True)
-
-        def accumulate(layer, k, start, depth, i, first=False):
-            at_rows = row_chunk(i)
+        gather(hidden, token_region, 5, 0, token_ready, nothing, TOKEN_AHEAD, unroll=True, between=token_hook)
+
+        def accumulate(layer, start, depth, at_rows, first=False):
             term = jnp.dot(
-                hidden[at_rows, pl.ds(multiple(start, kin), depth)],
-                w_in[layer, k, pl.ds(multiple(start, kin), depth), :],
+                hidden[at_rows, pl.ds(multiple(start, kc), depth)],
+                w_in[layer, pl.ds(multiple(start, kc), depth), :],
                 preferred_element_type=f32,
             )
-            acc[k, at_rows, :] = term if first else acc[k, at_rows, :] + term
+            acc[at_rows, :] = term if first else acc[at_rows, :] + term
 
         def wait_near(layer, k):
             ref = piece(layer, s, k)
             pltpu.make_async_copy(ref, ref, local_sem.at[1 + layer * pieces + k]).wait()
 
-        def near_in(layer, k, i):
-            accumulate(layer, k, base * kin, 2 * kin, i, first=True)
-
-        def far_in(layer, k):
-            for row, block in ((1, other), (2, far)):
-                w_wait(layer, k, row, block)
-
-            @pl.loop(0, CHUNKS)
-            def _(i):
-                accumulate(layer, k, 2 * (1 - half) * kin, 2 * kin, i)
-
-        tr = tile_rows(chunk_rows, 96)
-
-        def branch_columns(gg, tt, k):
-            return pl.ds(multiple(tt * parts * wide + gg * wide + k * sub, sub), sub)
-
-        def gate(layer, k, i):
+        def near_in(layer, at_rows):
+            accumulate(layer, base * kin, 2 * kin, at_rows, first=True)
+
+        def far_in(layer):
+            def add(start, depth):
+                @pl.loop(0, 4)
+                def _(i):
+                    accumulate(layer, start, depth, row_chunk(i, 4))
+
+            for k in pieces_in:
+                w_wait(layer, k, 1, other)
+            add(other * kin, kin)
+            for k in pieces_in:
+                w_wait(layer, k, 2, far)
+                add(far * kin + k * kc, kc)
+
+        tr = tile_rows(total // 10, 96)
+
+        def gate(layer, i):
             taps = [
-                conv_taps[n, layer : layer + 1, pl.ds(multiple(g * wide + k * sub, sub), sub)] for n in range(reach + 1)
+                conv_taps[n, layer : layer + 1, pl.ds(multiple(g * wide, wide), wide)] for n in range(reach + 1)
             ]
-            row_of = lax.broadcasted_iota(jnp.int32, (tr, sub), 0)
-
-            @pl.loop(0, chunk_rows // tr)
+            row_of = lax.broadcasted_iota(jnp.int32, (tr, wide), 0)
+            first = i * (total // BRANCH_CHUNKS)
+            sums = acc[pl.ds(multiple(jnp.maximum(first - 8, 0), 8), 8), wide:].astype(bf16).astype(f32)
+            unseen = HALO * (1 - half) - (first - 8) % part_rows
+            carry[...] = jnp.where(row_of[:8] < unseen, 0.0, sums[:, :wide] * sums[:, wide:])
+
+            @pl.loop(0, total // BRANCH_CHUNKS // tr)
             def _(q):
-                start = multiple(i * chunk_rows + q * tr, 16)
+                start = multiple(i * (total // BRANCH_CHUNKS) + q * tr, 16)
                 position = start % part_rows
-                sums = acc[k, pl.ds(start, tr), :].astype(bf16).astype(f32)
-                out_gate, in_gate, values = (sums[:, j * sub : (j + 1) * sub] for j in range(3))
+                sums = acc[pl.ds(start, tr), :].astype(bf16).astype(f32)
+                out_gate, in_gate, values = (sums[:, j * wide : (j + 1) * wide] for j in range(3))
                 gated = in_gate * values
                 gated = jnp.where(row_of < HALO * (1 - half) - position, 0.0, gated)
                 before = jnp.where(position == 0, 0.0, carry[...])
@@ -419,16 +484,7 @@
                             moved = jnp.where(row_of == j, before[8 - shift + j : 8 - shift + j + 1, :], moved)
                     conv = conv + taps[n] * moved
                 carry[...] = gated[tr - 8 :, :]
-                branch[pl.ds(start, tr), branch_columns(g, t, k)] = (out_gate * conv).astype(bf16)
-
-        def branches(layer, k, consume):
-            gather(
-                branch, lambda gg, tt, i: (row_chunk(i), branch_columns(gg, tt, k)),
-                CHUNKS, 1 + k, lambda i: gate(layer, k, i), consume, 2,
-            )
-
-        def sum_region(gg, tt, i):
-            return row_chunk(i), pl.ds(multiple(tt * ow + gg * owide, owide), owide)
+                branch[pl.ds(start, tr), branch_columns(g, t)] = (out_gate * conv).astype(bf16)
 
         def wait_out(layer):
             wait_near(layer, 2)
@@ -443,24 +499,25 @@
             return (residual_scale * kept + mixed.astype(bf16).astype(f32)).astype(bf16)
 
         def produce_sum(i):
-            raw[row_chunk(i), own_columns] = mix(0, row_chunk(i))
+            at_rows = row_chunk(i, SUM_CHUNKS)
+            raw[at_rows, own_columns] = mix(0, at_rows)
 
         strips = [slice(n, n + 128) for n in range(0, hidden.shape[1], 128)]
         ones[...] = jnp.ones_like(ones)
 
         def normalise(i):
-            means[...] = jnp.dot(raw[row_chunk(i), :], ones[...], preferred_element_type=f32) / ones.shape[0]
-
-            @pl.loop(0, chunk_rows // tr)
+            means[...] = jnp.dot(raw[row_chunk(i, SUM_CHUNKS), :], ones[...], preferred_element_type=f32) / ones.shape[0]
+
+            @pl.loop(0, total // SUM_CHUNKS // tr)
             def _(q):
-                there_rows = pl.ds(multiple(i * chunk_rows + q * tr, 16), tr)
+                there_rows = pl.ds(multiple(i * (total // SUM_CHUNKS) + q * tr, 16), tr)
                 here_rows = pl.ds(multiple(q * tr, 16), tr)
                 mean = means[here_rows, :]
-                total = jnp.zeros_like(mean)
+                squares = jnp.zeros_like(mean)
                 for strip in strips:
                     centered = raw[there_rows, strip].astype(f32) - mean
-                    total = total + centered * centered
-                scale = lax.rsqrt(jnp.sum(total, axis=1, keepdims=True) / ones.shape[0] + norm_eps)
+                    squares = squares + centered * centered
+                scale = lax.rsqrt(jnp.sum(squares, axis=1, keepdims=True) / ones.shape[0] + norm_eps)
                 scale = jnp.broadcast_to(scale, mean.shape)
                 for strip in strips:
                     centered = raw[there_rows, strip].astype(f32) - mean
@@ -474,33 +531,30 @@
 
         def consume_sum(i):
             normalise(i)
-            near_in(1, 0, i)
-
-            @pl.when(i == 0)
+            near_in(1, row_chunk(i, SUM_CHUNKS))
+
+            @pl.when(i == 2)
             def _():
-                send_pair(1, 1)
-
-            near_in(1, 1, i)
+                send_pair(1, 2)
 
         def first_branches(i):
-            near_in(0, 1, i)
-
-            @pl.when(i == CHUNKS - 1)
+            @pl.when(i == BRANCH_CHUNKS - 2)
             def _():
-                send_pair(0, 2)
+                send_pair(1, 0)
 
         for k in pieces_in:
             wait_near(0, k)
 
-        @pl.loop(0, CHUNKS)
+        @pl.loop(0, 4)
         def _(i):
-            near_in(0, 0, i)
-
-        far_in(0, 0)
-        branches(0, 0, first_branches)
-        far_in(0, 1)
-        branches(0, 1, nothing)
-        send_pair(1, 0)
+            near_in(0, row_chunk(i, 4))
+
+        far_in(0)
+        send_pair(0, 2)
+        gather(
+            branch, branch_region, BRANCH_CHUNKS, 1, lambda i: gate(0, i), first_branches, BRANCH_AHEAD
+        )
+        send_pair(1, 1)
         for k in range(1, lanes):
             copy(
                 own_scales, scales.at[:, pl.ds(multiple(((t + lanes - k) % lanes) * ow, ow), ow)],
@@ -509,12 +563,12 @@
         wait_out(0)
         for k in pieces_in:
             wait_near(1, k)
-        gather(raw, sum_region, CHUNKS, 0, produce_sum, consume_sum, 1)
-        far_in(1, 0)
-        send_pair(1, 2)
-        branches(1, 0, nothing)
-        far_in(1, 1)
-        branches(1, 1, nothing)
+        gather(raw, sum_region, SUM_CHUNKS, 0, produce_sum, consume_sum, SUM_AHEAD, via=SUM_VIA_END)
+        far_in(1)
+        gather(
+            branch, branch_region, BRANCH_CHUNKS, 2, lambda i: gate(1, i), nothing, BRANCH_AHEAD,
+            via=BRANCH_VIA_END,
+        )
         wait_out(1)
 
         def result_copy(j):
@@ -599,22 +653,22 @@
             pltpu.VMEM((total, depth), bf16),
             pltpu.VMEM((total, depth), bf16),
             pltpu.VMEM((total, channels), bf16),
-            pltpu.VMEM((LAYERS, 2, depth, 3 * wide // 2), bf16),
+            pltpu.VMEM((LAYERS, depth, 3 * wide), bf16),
             pltpu.VMEM((LAYERS, channels, owide), bf16),
-            pltpu.VMEM((2, total, 3 * wide // 2), f32),
-            pltpu.VMEM((8, wide // 2), f32),
+            pltpu.VMEM((total, 3 * wide), f32),
+            pltpu.VMEM((8, wide), f32),
             pltpu.VMEM((4, rows, owide), bf16),
             pltpu.VMEM((rows, ow), bf16),
             pltpu.VMEM((8, depth), f32),
             pltpu.VMEM((8, ow), f32),
             pltpu.VMEM((lanes, 8, rows), f32),
             pltpu.VMEM((depth, 128), bf16),
-            pltpu.VMEM((total // CHUNKS, 128), f32),
+            pltpu.VMEM((total // SUM_CHUNKS, 128), f32),
             dma((1 + 3 * LAYERS,)),
             dma((3, 3 * LAYERS)),
             dma((3, 3 * LAYERS)),
-            dma((3, 5, 7)),
-            dma((3, 5, 7)),
+            dma((3, max(5, SUM_CHUNKS, BRANCH_CHUNKS), 7)),
+            dma((3, max(5, SUM_CHUNKS, BRANCH_CHUNKS), 7)),
             dma((20,)),
             dma((20,)),
         ],

time: 273 us -> 247 us (0.905)
  Pallas kernels: 271 us -> 245 us
    pallas_call x1, Pallas kernels: 271 us -> 245 us  [mixer(): pl.pallas_call(mixer_kernel, out_shape=jax.ShapeDtypeStruct((rows, ow), b...]
where the time goes in v2:
time: 247 us
  Pallas kernels  245 us (99%)
    pallas_call x1, Pallas kernels, mixer(): pl.pallas_call(mixer_kernel, out_shape=jax.ShapeDtypeStruct((rows, ow), b...  245 us

profile of v2, /device:TPU:0, one launch (start us, length us, event | category | flops | bytes accessed | tf_op | source)
XLA Modules:
  0.0 246.7 jit_solution(5459259854813175090)
XLA Ops:
  0.0 244.6 %shard_map.82 = bf16[384,1024]{1,0:T(8,128)(2,1)} custom-call(bf16[384,1024]{1,0:T(8,128)(2,1)} %tokens.1, bf16[2,1024,512]{2,1,0:T(8,128)(2,1)} %proj_b.1, bf16[2,1024,512]{2,1,0:T(8,128)(2,1)} %proj_c.1, bf16[2,1024,512]{2,1,0:T(8,128)(2,1)} %proj_x.1, bf16[2,512,1024]{2,1,0:T(8,128)(2,1)} %proj_out.1, f32[3,2,512]{2,1,0:T(2,128)} %bitcast.1, ...), custom_call_target="tpu_custom_call" | custom-call | tf_op jit(solution)/shard_map/pallas_call | solution.py:647
  244.6 2.1 copy.10

commit v3 on v2

--- a/solution.py
+++ b/solution.py
@@ -112,7 +112,10 @@
 SUM_CHUNKS = 5
 BRANCH_AHEAD = 1
 TOKEN_AHEAD = 1
-TOKEN_HOOK = 2
+OWN_HOOK = 2
+OUT_EARLY = False
+OUT_HOOK = 2
+NEXT_HOOK = 2
 SUM_AHEAD = 1
 BRANCH_VIA_END = 1
 SUM_VIA_END = 1
@@ -244,10 +247,11 @@
             for j in range(2):
                 end_tokens(j).wait_send()
 
-        send_tokens()
         for layer, k in order:
             send_own(layer, k, (g, mid, t), 0)
             w_wait(layer, k, 0, s, sent=True)
+            if (layer, k) == (0, 0):
+                send_tokens()
 
         def pass_through(buffer, region, count, family, via):
             def transfer(owner, i, role, kind, device):
@@ -279,8 +283,7 @@
         there = (g, other, t)
 
         greet(lane_peers + [(1 - g, mid, t), there] + [(gg, end, t) for gg in range(parts)])
-        for k in pieces_in:
-            send_own(0, k, there, 1)
+        send_own(0, 0, there, 1)
         mine = hidden.at[token_rows(mid - base), pl.ds(multiple(t * ow, ow), ow)]
         pltpu.make_async_copy(tokens, mine, local_sem.at[0]).start()
         for layer, k in order:
@@ -418,8 +421,10 @@
                 copy(slab, slab, small_send.at[3 * (i - 3)], small_recv.at[3 * (i - 3)], me).wait_recv()
 
         def token_hook(i):
-            if i == TOKEN_HOOK:
+            if i == 1:
                 relay(0, 0)
+            if i == OWN_HOOK:
+                send_own(0, 1, there, 1)
             if i == 4:
                 relay(0, 1)
 
@@ -533,12 +538,12 @@
             normalise(i)
             near_in(1, row_chunk(i, SUM_CHUNKS))
 
-            @pl.when(i == 2)
+            @pl.when(i == OUT_HOOK)
             def _():
                 send_pair(1, 2)
 
         def first_branches(i):
-            @pl.when(i == BRANCH_CHUNKS - 2)
+            @pl.when(i == BRANCH_CHUNKS - NEXT_HOOK)
             def _():
                 send_pair(1, 0)
 
@@ -549,8 +554,11 @@
         def _(i):
             near_in(0, row_chunk(i, 4))
 
+        if OUT_EARLY:
+            send_pair(0, 2)
         far_in(0)
-        send_pair(0, 2)
+        if not OUT_EARLY:
+            send_pair(0, 2)
         gather(
             branch, branch_region, BRANCH_CHUNKS, 1, lambda i: gate(0, i), first_branches, BRANCH_AHEAD
         )

time: 247 us -> 235 us (0.951)
  Pallas kernels: 245 us -> 233 us
    pallas_call x1, Pallas kernels: 245 us -> 233 us  [mixer(): pl.pallas_call(mixer_kernel, out_shape=jax.ShapeDtypeStruct((rows, ow), b...]
where the time goes in v3:
time: 235 us
  Pallas kernels  233 us (99%)
    pallas_call x1, Pallas kernels, mixer(): pl.pallas_call(mixer_kernel, out_shape=jax.ShapeDtypeStruct((rows, ow), b...  233 us

profile of v3, /device:TPU:0, one launch (start us, length us, event | category | flops | bytes accessed | tf_op | source)
XLA Modules:
  0.0 234.9 jit_solution(17887376000007609213)
XLA Ops:
  0.0 232.8 %shard_map.82 = bf16[384,1024]{1,0:T(8,128)(2,1)} custom-call(bf16[384,1024]{1,0:T(8,128)(2,1)} %tokens.1, bf16[2,1024,512]{2,1,0:T(8,128)(2,1)} %proj_b.1, bf16[2,1024,512]{2,1,0:T(8,128)(2,1)} %proj_c.1, bf16[2,1024,512]{2,1,0:T(8,128)(2,1)} %proj_x.1, bf16[2,512,1024]{2,1,0:T(8,128)(2,1)} %proj_out.1, f32[3,2,512]{2,1,0:T(2,128)} %bitcast.1, ...), custom_call_target="tpu_custom_call" | custom-call | tf_op jit(solution)/shard_map/pallas_call | solution.py:655
  232.9 2.1 copy.10

commit v4 on v3

--- a/solution.py
+++ b/solution.py
@@ -115,6 +115,7 @@
 OWN_HOOK = 2
 OUT_EARLY = False
 OUT_HOOK = 2
+SUM_HOOK = 3
 NEXT_HOOK = 2
 SUM_AHEAD = 1
 BRANCH_VIA_END = 1
@@ -307,7 +308,7 @@
                 small_send.at[4 + k], small_recv.at[4 + k], (g, s, (t + k) % lanes),
             ).start()
 
-        def gather(buffer, region, count, family, produce, consume, ahead, unroll=False, via=0, between=None):
+        def gather(buffer, region, count, family, produce, consume, ahead, unroll=False, via=0, between=None, begun=0):
             def at(device, i):
                 return buffer.at[region(device[0], device[2], i)]
 
@@ -348,7 +349,7 @@
                 transfer(me, i, 3, 0, (g, end, t)).start()
                 transfer(me, i, 3, 2, pp).start()
             count = count - via
-            for i in range(ahead):
+            for i in range(begun, ahead):
                 send(i)
             if unroll:
                 for i in range(count + 1):
@@ -542,7 +543,18 @@
             def _():
                 send_pair(1, 2)
 
+        def begin_sums():
+            wait_out(0)
+            produce_sum(0)
+            ref = raw.at[sum_region(g, t, 0)]
+            for role, kind, device in ((0, 0, up), (1, 1, vp), (3, 2, pp)):
+                copy(ref, ref, ag_send.at[0, 0, kind], ag_recv.at[0, 0, role], device).start()
+
         def first_branches(i):
+            @pl.when(i == SUM_HOOK)
+            def _():
+                begin_sums()
+
             @pl.when(i == BRANCH_CHUNKS - NEXT_HOOK)
             def _():
                 send_pair(1, 0)
@@ -568,10 +580,9 @@
                 own_scales, scales.at[:, pl.ds(multiple(((t + lanes - k) % lanes) * ow, ow), ow)],
                 small_send.at[4 + k], small_recv.at[4 + k], me,
             ).wait()
-        wait_out(0)
         for k in pieces_in:
             wait_near(1, k)
-        gather(raw, sum_region, SUM_CHUNKS, 0, produce_sum, consume_sum, SUM_AHEAD, via=SUM_VIA_END)
+        gather(raw, sum_region, SUM_CHUNKS, 0, produce_sum, consume_sum, SUM_AHEAD, via=SUM_VIA_END, begun=1)
         far_in(1)
         gather(
             branch, branch_region, BRANCH_CHUNKS, 2, lambda i: gate(1, i), nothing, BRANCH_AHEAD,

time: 235 us -> 234 us (level)
  no operation moved by 1% of the time
where the time goes in v4:
time: 234 us
  Pallas kernels  231 us (99%)
    pallas_call x1, Pallas kernels, mixer(): pl.pallas_call(mixer_kernel, out_shape=jax.ShapeDtypeStruct((rows, ow), b...  231 us

profile of v4, /device:TPU:0, one launch (start us, length us, event | category | flops | bytes accessed | tf_op | source)
XLA Modules:
  0.0 233.6 jit_solution(2919383308082524537)
XLA Ops:
  0.0 231.5 %shard_map.82 = bf16[384,1024]{1,0:T(8,128)(2,1)} custom-call(bf16[384,1024]{1,0:T(8,128)(2,1)} %tokens.1, bf16[2,1024,512]{2,1,0:T(8,128)(2,1)} %proj_b.1, bf16[2,1024,512]{2,1,0:T(8,128)(2,1)} %proj_c.1, bf16[2,1024,512]{2,1,0:T(8,128)(2,1)} %proj_x.1, bf16[2,512,1024]{2,1,0:T(8,128)(2,1)} %proj_out.1, f32[3,2,512]{2,1,0:T(2,128)} %bitcast.1, ...), custom_call_target="tpu_custom_call" | custom-call | tf_op jit(solution)/shard_map/pallas_call | solution.py:666
  231.5 2.1 copy.10
